TPU v7x, 32 devices: a whole 2x2x4 slice. The times are simulated.
32 devices in a mesh: sp: 16 (over z, y, x), tp: 2 (over core).
Axes of the slice: x: 2, y: 2, z: 4, core: 2. Of those that a mesh axis runs over, the one named last changes fastest.
Arguments:
- stream: bfloat16 [2048, 2048], P('sp', 'tp'), may hold values from -14 to 14
- queries: bfloat16 [2048, 2048], P('sp', 'tp'), may hold values from -6 to 6
- key_rows: bfloat16 [2048, 2048], P('sp', 'tp'), may hold values from -6 to 6
- values: bfloat16 [2048, 2048], P('sp', 'tp'), may hold values from -6 to 6
- out_gate: bfloat16 [2048, 2048], P('sp', 'tp'), may hold values from -6 to 6
- in_gate: float32 [16, 2048], P('tp', 'sp'), may hold values from -4 to 120
- forget_gate: float32 [16, 2048], P('tp', 'sp'), may hold values from -1 to 20
- head_gain: float32 [2048], P('tp'), may hold values from 0.1 to 1.9
- w_out: bfloat16 [2048, 2048], P('tp'), may hold values from -0.30935922 to 0.30935922
- norm_gains: bfloat16 [3, 2048], P(None, 'tp'), may hold values from 0.099609375 to 1.8984375
- w_gate: bfloat16 [2048, 5632], P('sp', 'tp'), may hold values from -0.125 to 0.125
- w_up: bfloat16 [2048, 5632], P('sp', 'tp'), may hold values from -0.125 to 0.125
- w_down: bfloat16 [5632, 2048], P('tp', 'sp'), may hold values from -0.18655063 to 0.18655063
Outputs:
- result: bfloat16 [2048, 2048], P('sp', 'tp')
All inputs are finite; a program needn't handle non-finite values.
Results may differ from a plain program's by a relative error of at most 0.012.
Values may be sent and summed in bfloat16 or wider, within the bound.
No kernel may reach another device: no remote copies, remote signals or barrier semaphores. Data moves between devices by JAX's collectives and lax.ppermute only.
A program may use at most 128 MiB of HBM per device.

v0:
```python
import jax
import jax.numpy as jnp
from jax import lax
from jax.sharding import PartitionSpec as P

D = 2048
BLOCK = 128
EPS = 1e-06


def carried_in(value, axis, combine, identity):
    peers, position = (lax.axis_size(axis), lax.axis_index(axis))
    everything = jax.tree.map(lambda part: lax.all_gather(part, axis), value)
    start = jax.tree.map(
        lambda part, zero: jnp.broadcast_to(jnp.asarray(zero, part.dtype), part.shape),
        value,
        identity,
    )

    def turn(k, before):
        reached = k < position
        new = combine(before, jax.tree.map(lambda part: part[k], everything))
        return jax.tree.map(lambda a, b: jnp.where(reached, a, b), new, before)

    return lax.fori_loop(0, peers, turn, start)


def join_states(earlier, later):
    total_early, summit_early, memory_early = earlier
    total_late, summit_late, memory_late = later
    summit = jnp.maximum(total_late + summit_early, summit_late)
    scale_early = jnp.exp(total_late + summit_early - summit)
    scale_late = jnp.exp(summit_late - summit)
    memory = scale_early[:, None, None] * memory_early + scale_late[:, None, None] * memory_late
    return (total_early + total_late, summit, memory)


def cell_block(queries, key_rows, values, in_gate, forget_gate):
    highest = lax.Precision.HIGHEST
    tokens_here = queries.shape[0]
    heads_here = in_gate.shape[0]
    head_dim = queries.shape[1] // heads_here
    blocks = tokens_here // BLOCK
    key_scale = head_dim ** (-0.5)
    log_forget = jax.nn.log_sigmoid(forget_gate)
    cumulative = jnp.cumsum(log_forget, axis=1)
    total_log = cumulative[:, -1]
    toward = total_log[:, None] - cumulative + in_gate
    summit = jnp.max(toward, axis=1)
    weight_key = jnp.exp(toward - summit[:, None])
    key_scaled = key_rows.astype(jnp.float32).reshape(tokens_here, heads_here, head_dim) * key_scale
    value_float = values.astype(jnp.float32).reshape(tokens_here, heads_here, head_dim)
    weighted = key_scaled * weight_key.T[:, :, None]
    memory_dev = jnp.einsum("shd,she->hde", weighted, value_float, precision=highest)
    identity = (jnp.zeros_like(total_log), jnp.full_like(summit, -1e30), jnp.zeros_like(memory_dev))
    prior_total, prior_summit, prior_memory = carried_in(
        (total_log, summit, memory_dev), "sp", join_states, identity
    )
    start_summit = jnp.maximum(prior_total, prior_summit)
    carry_scale = jnp.exp(prior_summit - start_summit)
    start_memory = carry_scale[:, None, None] * prior_memory
    query_blocks = queries.reshape(blocks, BLOCK, heads_here, head_dim)
    key_blocks = key_rows.reshape(blocks, BLOCK, heads_here, head_dim)
    value_blocks = values.reshape(blocks, BLOCK, heads_here, head_dim)
    keyf_blocks = key_scaled.reshape(blocks, BLOCK, heads_here, head_dim)
    forget_blocks = log_forget.reshape(heads_here, blocks, BLOCK).transpose(1, 0, 2)
    input_blocks = in_gate.reshape(heads_here, blocks, BLOCK).transpose(1, 0, 2)
    causal = jnp.tril(jnp.ones((BLOCK, BLOCK), dtype=bool))

    def advance(carried, inputs):
        memory, stabil = carried
        query_blk, key_blk, value_blk, keyf_blk, forget_blk, input_blk = inputs
        cumul_blk = jnp.cumsum(forget_blk, axis=-1)
        within = jnp.where(
            causal, cumul_blk[:, :, None] - cumul_blk[:, None, :] + input_blk[:, None, :], -jnp.inf
        )
        across = cumul_blk + stabil[:, None]
        stable = jnp.maximum(across, jnp.max(within, axis=-1))
        weight_in = jnp.exp(within - stable[:, :, None])
        weight_out = jnp.exp(across - stable)
        raw_scores = (
            jnp.einsum("thd,shd->hts", query_blk, key_blk, preferred_element_type=jnp.float32)
            * key_scale
        )
        scores = raw_scores * weight_in
        probs_low = scores.astype(jnp.bfloat16)
        query_float = query_blk.astype(jnp.float32)
        output = jnp.einsum(
            "hts,shd->htd", probs_low, value_blk, preferred_element_type=jnp.float32
        )
        output = output + weight_out[:, :, None] * jnp.einsum(
            "thd,hde->hte", query_float, memory, precision=highest
        )
        last_sum = cumul_blk[:, -1]
        toward_blk = last_sum[:, None] - cumul_blk + input_blk
        stabil_new = jnp.maximum(last_sum + stabil, jnp.max(toward_blk, axis=-1))
        decay_now = jnp.exp(last_sum + stabil - stabil_new)
        weight_blk = jnp.exp(toward_blk - stabil_new[:, None])
        weighted_blk = keyf_blk * weight_blk.T[:, :, None]
        memory_new = decay_now[:, None, None] * memory + jnp.einsum(
            "shd,she->hde", weighted_blk, value_blk.astype(jnp.float32), precision=highest
        )
        return ((memory_new, stabil_new), output.transpose(1, 0, 2))

    _, outputs = lax.scan(
        advance,
        (start_memory, start_summit),
        (query_blocks, key_blocks, value_blocks, keyf_blocks, forget_blocks, input_blocks),
    )
    return outputs.reshape(tokens_here, heads_here, head_dim)


def shards(
    stream,
    queries,
    key_rows,
    values,
    out_gate,
    in_gate,
    forget_gate,
    head_gain,
    w_out,
    norm_gains,
    w_gate,
    w_up,
    w_down,
):
    tokens_here = queries.shape[0]
    cell = cell_block(queries, key_rows, values, in_gate, forget_gate)
    normed_cell = cell * lax.rsqrt(jnp.mean(cell * cell, axis=-1, keepdims=True) + EPS)
    mixed = (
        normed_cell.reshape(tokens_here, -1)
        * head_gain
        * jax.nn.sigmoid(out_gate.astype(jnp.float32))
    ).astype(jnp.bfloat16)
    partial_mix = jnp.dot(mixed, w_out, preferred_element_type=jnp.float32)
    own_gains = norm_gains.astype(jnp.float32)
    mix_sum = lax.psum_scatter(
        partial_mix.astype(jnp.bfloat16), "tp", scatter_dimension=1, tiled=True
    ).astype(jnp.float32)
    mix_squares = lax.psum(jnp.sum(mix_sum * mix_sum, axis=1), "tp")
    mix_norm = mix_sum * lax.rsqrt(mix_squares / D + EPS)[:, None] * own_gains[0]
    after_mix = (stream.astype(jnp.float32) + mix_norm).astype(jnp.bfloat16)
    kept_rows = after_mix.astype(jnp.float32)
    resid_squares = lax.psum(jnp.sum(kept_rows * kept_rows, axis=1), "tp")
    normed = (kept_rows * lax.rsqrt(resid_squares / D + EPS)[:, None] * own_gains[1]).astype(
        jnp.bfloat16
    )
    normed_all = lax.all_gather(normed, "tp", axis=1, tiled=True)
    gate_part = jnp.dot(
        normed_all,
        lax.all_gather(w_gate, "sp", axis=0, tiled=True),
        preferred_element_type=jnp.float32,
    )
    up_part = jnp.dot(
        normed_all,
        lax.all_gather(w_up, "sp", axis=0, tiled=True),
        preferred_element_type=jnp.float32,
    )
    hidden = (jax.nn.silu(gate_part) * up_part).astype(jnp.bfloat16)
    ffn_terms = jnp.dot(
        hidden, lax.all_gather(w_down, "sp", axis=1, tiled=True), preferred_element_type=jnp.float32
    )
    ffn_sum = lax.psum_scatter(
        ffn_terms.astype(jnp.bfloat16), "tp", scatter_dimension=1, tiled=True
    ).astype(jnp.float32)
    ffn_squares = lax.psum(jnp.sum(ffn_sum * ffn_sum, axis=1), "tp")
    ffn_norm = ffn_sum * lax.rsqrt(ffn_squares / D + EPS)[:, None] * own_gains[2]
    return (kept_rows + 0.5 * ffn_norm).astype(jnp.bfloat16)


def solution(mesh):
    in_specs = (
        P("sp", "tp"),
        P("sp", "tp"),
        P("sp", "tp"),
        P("sp", "tp"),
        P("sp", "tp"),
        P("tp", "sp"),
        P("tp", "sp"),
        P("tp"),
        P("tp", None),
        P(None, "tp"),
        P("sp", "tp"),
        P("sp", "tp"),
        P("tp", "sp"),
    )
    out_specs = P("sp", "tp")
    return jax.shard_map(shards, mesh=mesh, in_specs=in_specs, out_specs=out_specs, check_vma=False)
```

profile of v0, /device:TPU:0, one launch (start us, length us, event | category | flops | bytes accessed | tf_op | source)
XLA Modules:
  0.0 661.8 jit_solution(8286072181642715078)
XLA Ops:
  11.6 1.5 fusion.24
  13.3 1.2 dynamic-slice.2
  15.6 44.4 %all-reduce.2 = (f32[128]{0:T(128)S(1)}, f32[128]{0:T(128)S(1)}) all-reduce(f32[128]{0:T(128)S(1)} %dynamic-update-slice, f32[128]{0:T(128)S(1)} %dynamic-update-slice.1), channel_id=2, replica_groups=mesh['sp'=16,'tp'=2] {'sp'}, use_global_device_ids=true, to_apply=%add | all-reduce | flops 256 | bytes 2048
  61.3 67.6 %all-gather.14.cloned.1.call-done = f32[128,128,128]{2,1,0:T(8,128)} async-done(((f32[8,128,128]{2,1,0:T(8,128)}), f32[128,128,128]{2,1,0:T(8,128)}) %all-gather.14.cloned.1.call-update) | async-done | bytes 8388624 | tf_op jit(solution)/shard_map/all_gather | solution.py:13
  128.8 20.3 %while.5 = (s32[]{:T(128)}, f32[8]{0:T(128)S(1)}, f32[8]{0:T(128)S(1)}, f32[8,128,128]{2,1,0:T(8,128)S(1)}, s32[]{:T(128)}, /*index=5*/f32[16,8]{1,0:T(8,128)S(1...) while((s32[]{:T(128)}, f32[8]{0:T(128)S(1)}, f32[8]{0:T(128)S(1)}, ...), condition=%wide.region_3.4_spmd.clone, body=%wide.region_2.3_spmd.clone.sunk | while | flops 655452 | bytes 1573449 | solution.py:25
  136.5 1.2 fusion.70
  137.8 1.2 fusion.70
  139.1 1.2 fusion.70
  140.3 1.2 fusion.70
  141.6 1.2 fusion.70
  150.9 3.8 convolution_convert_fusion.1
  156.7 4.3 reduce-scatter.3.cloned.1.call-done
  162.1 2.5 psum.21
  164.5 1.2 fusion.17
  165.8 2.5 psum.22
  168.4 2.2 all_gather.32
  170.6 135.7 %all-gather.8.cloned.1.call-done = bf16[2048,2816]{1,0:T(8,128)(2,1)} async-done(((bf16[128,2816]{1,0:T(8,128)(2,1)}), bf16[2048,2816]{1,0:T(8,128)(2,1)}) %all-gather.8.cloned.1.call-update) | async-done | bytes 11534352 | tf_op jit(solution)/shard_map/all_gather | solution.py:152
  306.3 5.9 fusion.57
  312.2 136.3 %all-gather.10.cloned.1.call-done = bf16[2048,2816]{1,0:T(8,128)(2,1)} async-done(((bf16[128,2816]{1,0:T(8,128)(2,1)}), bf16[2048,2816]{1,0:T(8,128)(2,1)}) %all-gather.10.cloned.1.call-update) | async-done | bytes 11534352 | tf_op jit(solution)/shard_map/all_gather | solution.py:157
  448.5 182.8 %all-gather.12.cloned.1.call-done = bf16[2816,2048]{1,0:T(8,128)(2,1)} async-done(((bf16[2816,128]{1,0:T(8,128)(2,1)}), bf16[2816,2048]{1,0:T(8,128)(2,1)}) %all-gather.12.cloned.1.call-update) | async-done | bytes 11534352 | tf_op jit(solution)/shard_map/all_gather | solution.py:162
  631.3 11.9 %convolution_convert_fusion = bf16[128,2048]{1,0:T(8,128)(2,1)} fusion(bf16[2816,2048]{1,0:T(8,128)(2,1)} %all-gather.12.cloned.1.call-done, bf16[128,2048]{1,0:T(8,128)(2,1)S(1)} %all_gather.32, bf16[2048,2816]{1,0:T(8,128)(2,1)} %all-gather.10.cloned.1.call-done, f32[128,2816]{1,0:T(8,128)S(1)} %fusion.57), kind=kOutput, calls=%fused_computation.16 | convolution fusion | flops 2955214848 | bytes 25559040 | tf_op jit(solution)/shard_map/dot_general | solution.py:161
  643.2 6.3 reduce-scatter.5.cloned.1.call-done
  650.6 2.5 psum.23
  653.1 1.8 fusion.20
  (100 shorter events, 26.6 us)
Async XLA Ops:
  6.5 142.8 %copy-start = (bf16[128,1024]{1,0:T(8,128)(2,1)S(1)}, bf16[128,1024]{1,0:T(8,128)(2,1)}, u32[]{:S(2)}) copy-start(bf16[128,1024]{1,0:T(8,128)(2,1)} %param.16) | copy-start | bytes 786436
  6.5 122.3 %all-gather.14.cloned.1.call-start = ((), (), s32[]{:S(2)}) async-start(), calls=%async_computation.7 | async-start | bytes 8912896 | tf_op jit(solution)/shard_map/all_gather | solution.py:13
  13.2 147.8 %reduce-scatter.3.cloned.1.call-start = ((), (), s32[]{:S(2)}) async-start(), calls=%async_computation.2 | async-start | bytes 786432 | tf_op jit(solution)/shard_map/reduce_scatter | solution.py:138
  128.8 21.2 %copy-start.2 = (f32[8,128]{1,0:T(8,128)S(1)}, f32[8,128]{1,0:T(8,128)}, u32[]{:S(2)}) copy-start(f32[8,128]{1,0:T(8,128)} %param.20) | copy-start | bytes 12292
  149.2 1.7 copy-start.4
  149.2 1.7 copy-start.5
  150.9 5.8 copy-start.3
  150.9 13.6 %copy-start.1 = (bf16[128,1024]{1,0:T(8,128)(2,1)S(1)}, bf16[128,1024]{1,0:T(8,128)(2,1)}, u32[]{:S(2)}) copy-start(bf16[128,1024]{1,0:T(8,128)(2,1)} %param.15) | copy-start | bytes 786436
  154.7 151.6 %all-gather.8.cloned.1.call-start = ((), (), s32[]{:S(2)}) async-start(), calls=%async_computation.3 | async-start | bytes 12255232 | tf_op jit(solution)/shard_map/all_gather | solution.py:152
  155.5 293.1 %all-gather.10.cloned.1.call-start = ((), (), s32[]{:S(2)}) async-start(), calls=%async_computation.4 | async-start | bytes 12255232 | tf_op jit(solution)/shard_map/all_gather | solution.py:157
  156.0 475.3 %all-gather.12.cloned.1.call-start = ((), (), s32[]{:S(2)}) async-start(), calls=%async_computation.5 | async-start | bytes 12255232 | tf_op jit(solution)/shard_map/all_gather | solution.py:162
  156.6 492.9 %reduce-scatter.5.cloned.1.call-start = ((), (), s32[]{:S(2)}) async-start(), calls=%async_computation.6 | async-start | bytes 786432 | tf_op jit(solution)/shard_map/reduce_scatter | solution.py:164
Sparse Core Ops, SparseCore 0:
  13.3 115.4 all-gather.13
  154.8 6.0 reduce-scatter.2
  163.7 142.4 all-gather.7
  308.9 139.5 all-gather.9
  451.1 180.2 all-gather.11
  643.4 6.1 reduce-scatter.4
where the time goes:
time: 663 us; the launch traced here: 662 us
  waiting for transfers between devices  535 us (81%)
  blocking collectives  53.9 us (8%)
  other arithmetic  29.2 us (4%)
  matrix products  24.3 us (4%)
  between operations  14.3 us (2%)
    all_gather x1, waiting for transfers between devices, shards(): lax.all_gather(w_down, 'sp', axis=1, tiled=True)  183 us
    all_gather x1, waiting for transfers between devices, shards(): lax.all_gather(w_up, 'sp', axis=0, tiled=True)  136 us
    all_gather x1, waiting for transfers between devices, shards(): lax.all_gather(w_gate, 'sp', axis=0, tiled=True)  136 us
    all_gather x1, waiting for transfers between devices, carried_in(): everything = jax.tree.map(lambda part: lax.all_gather(part, axis), value)  67.6 us
    unnamed x1, blocking collectives  44.4 us
    select_n x16, other arithmetic, turn(): return jax.tree.map(lambda a, b: jnp.where(reached, a, b), new, before)  19.2 us
  transfers between devices with their start and end apart: 6, of which 6 were waited for; matrix products, arithmetic and copies ran while one was open for 2% of the time, Pallas kernels for 0%

commit v1 on v0

--- a/solution.py
+++ b/solution.py
@@ -159,7 +159,9 @@
     )
     hidden = (jax.nn.silu(gate_part) * up_part).astype(jnp.bfloat16)
     ffn_terms = jnp.dot(
-        hidden, lax.all_gather(w_down, "sp", axis=1, tiled=True), preferred_element_type=jnp.float32
+        hidden,
+        jnp.concatenate(lax.all_gather(w_down, "sp"), axis=1),
+        preferred_element_type=jnp.float32,
     )
     ffn_sum = lax.psum_scatter(
         ffn_terms.astype(jnp.bfloat16), "tp", scatter_dimension=1, tiled=True

time: 663 us -> 624 us (0.941)
  waiting for transfers between devices: 535 us -> 479 us
  local copies, waits for them, and re-layouts: 4.52 us -> 19.6 us
    all_gather x1, waiting for transfers between devices: 183 us -> 136 us  [shards(): lax.all_gather(w_down, 'sp')]
    reshape x0 -> x1, local copies, waits for them, and re-layouts: none -> 15.1 us  [shards(): jnp.concatenate(lax.all_gather(w_down, 'sp'), axis=1)]
    all_gather x1, waiting for transfers between devices: 136 us -> 127 us  [shards(): lax.all_gather(w_gate, 'sp', axis=0, tiled=True)]
  transfers between devices with their start and end apart: 6 -> 6, of which waited for: 6 -> 6; matrix products, arithmetic and copies ran while one was open for 2% -> 4% of each run, Pallas kernels for 0% -> 0%
where the time goes in v1:
time: 624 us; the launch traced here: 623 us
  waiting for transfers between devices  479 us (77%)
  blocking collectives  53.9 us (9%)
  other arithmetic  29.2 us (5%)
  matrix products  25.7 us (4%)
  local copies, waits for them, and re-layouts  19.6 us (3%)
  between operations  14.3 us (2%)
    all_gather x1, waiting for transfers between devices, shards(): lax.all_gather(w_up, 'sp', axis=0, tiled=True)  136 us
    all_gather x1, waiting for transfers between devices, shards(): lax.all_gather(w_down, 'sp')  136 us
    all_gather x1, waiting for transfers between devices, shards(): lax.all_gather(w_gate, 'sp', axis=0, tiled=True)  127 us
    all_gather x1, waiting for transfers between devices, carried_in(): everything = jax.tree.map(lambda part: lax.all_gather(part, axis), value)  67.6 us
    unnamed x1, blocking collectives  44.4 us
    select_n x16, other arithmetic, turn(): return jax.tree.map(lambda a, b: jnp.where(reached, a, b), new, before)  19.2 us
    reshape x1, local copies, waits for them, and re-layouts, shards(): jnp.concatenate(lax.all_gather(w_down, 'sp'), axis=1)  15.1 us
    dot_general x1, matrix products, shards(): jnp.dot(hidden, jnp.concatenate(lax.all_gather(w_down, 'sp'), axis=1), pr...  13.2 us
  transfers between devices with their start and end apart: 6, of which 6 were waited for; matrix products, arithmetic and copies ran while one was open for 4% of the time, Pallas kernels for 0%

profile of v1, /device:TPU:0, one launch (start us, length us, event | category | flops | bytes accessed | tf_op | source)
XLA Modules:
  0.0 622.5 jit_solution(3383738859838440461)
XLA Ops:
  11.7 1.5 fusion.24
  13.3 1.2 dynamic-slice.2
  15.7 44.4 %all-reduce.2 = (f32[128]{0:T(128)S(1)}, f32[128]{0:T(128)S(1)}) all-reduce(f32[128]{0:T(128)S(1)} %dynamic-update-slice, f32[128]{0:T(128)S(1)} %dynamic-update-slice.1), channel_id=2, replica_groups=mesh['sp'=16,'tp'=2] {'sp'}, use_global_device_ids=true, to_apply=%add | all-reduce | flops 256 | bytes 2048
  61.3 67.6 %all-gather.13.cloned.1.call-done = f32[128,128,128]{2,1,0:T(8,128)} async-done(((f32[8,128,128]{2,1,0:T(8,128)}), f32[128,128,128]{2,1,0:T(8,128)}) %all-gather.13.cloned.1.call-update) | async-done | bytes 8388624 | tf_op jit(solution)/shard_map/all_gather | solution.py:13
  128.9 20.3 %while.5 = (s32[]{:T(128)}, f32[8]{0:T(128)S(1)}, f32[8]{0:T(128)S(1)}, f32[8,128,128]{2,1,0:T(8,128)S(1)}, s32[]{:T(128)}, /*index=5*/f32[16,8]{1,0:T(8,128)S(1...) while((s32[]{:T(128)}, f32[8]{0:T(128)S(1)}, f32[8]{0:T(128)S(1)}, ...), condition=%wide.region_3.4_spmd.clone, body=%wide.region_2.3_spmd.clone.sunk | while | flops 655452 | bytes 1573449 | solution.py:25
  128.9 1.2 fusion.70
  130.2 1.2 fusion.70
  131.5 1.2 fusion.70
  132.7 1.2 fusion.70
  150.9 3.8 convolution_convert_fusion.1
  156.7 4.3 reduce-scatter.3.cloned.1.call-done
  162.1 2.5 psum.21
  164.6 1.2 fusion.17
  165.8 2.5 psum.22
  168.4 2.2 all_gather.35
  170.6 135.7 %all-gather.15.cloned.1.call-done = bf16[45056,128]{1,0:T(8,128)(2,1)} async-done(((bf16[2816,128]{1,0:T(8,128)(2,1)}), bf16[45056,128]{1,0:T(8,128)(2,1)}) %all-gather.15.cloned.1.call-update) | async-done | bytes 11534352 | tf_op jit(solution)/shard_map/all_gather | solution.py:163
  306.3 15.1 %copy.43 = bf16[2816,16,128]{0,2,1:T(8,128)(2,1)} copy(bf16[2816,16,128]{2,0,1:T(8,128)(2,1)} %bitcast.78) | data formatting | bytes 23068672 | tf_op jit(solution)/shard_map/reshape | solution.py:163
  321.4 127.1 %all-gather.9.cloned.1.call-done = bf16[2048,2816]{1,0:T(8,128)(2,1)} async-done(((bf16[128,2816]{1,0:T(8,128)(2,1)}), bf16[2048,2816]{1,0:T(8,128)(2,1)}) %all-gather.9.cloned.1.call-update) | async-done | bytes 11534352 | tf_op jit(solution)/shard_map/all_gather | solution.py:152
  448.5 5.9 fusion.57
  454.5 136.3 %all-gather.11.cloned.1.call-done = bf16[2048,2816]{1,0:T(8,128)(2,1)} async-done(((bf16[128,2816]{1,0:T(8,128)(2,1)}), bf16[2048,2816]{1,0:T(8,128)(2,1)}) %all-gather.11.cloned.1.call-update) | async-done | bytes 11534352 | tf_op jit(solution)/shard_map/all_gather | solution.py:157
  590.8 13.2 %convolution_convert_fusion = bf16[128,2048]{1,0:T(8,128)(2,1)} fusion(bf16[2816,2048]{0,1:T(8,128)(2,1)} %bitcast.79, bf16[128,2048]{1,0:T(8,128)(2,1)S(1)} %all_gather.35, bf16[2048,2816]{1,0:T(8,128)(2,1)} %all-gather.11.cloned.1.call-done, f32[128,2816]{1,0:T(8,128)S(1)} %fusion.57), kind=kOutput, calls=%fused_computation.16 | convolution fusion | flops 2955214848 | bytes 25559040 | tf_op jit(solution)/shard_map/dot_general | solution.py:161
  604.0 6.3 %reduce-scatter.5.cloned.1.call-done = bf16[128,1024]{1,0:T(8,128)(2,1)} async-done(((bf16[128,2048]{1,0:T(8,128)(2,1)}), bf16[128,1024]{1,0:T(8,128)(2,1)}) %reduce-scatter.5.cloned.1.call-update) | async-done | bytes 262160 | tf_op jit(solution)/shard_map/reduce_scatter | solution.py:166
  611.4 2.5 psum.23
  613.9 1.8 fusion.20
  (103 shorter events, 27.9 us)
Async XLA Ops:
  6.5 142.9 %copy-start = (bf16[128,1024]{1,0:T(8,128)(2,1)S(1)}, bf16[128,1024]{1,0:T(8,128)(2,1)}, u32[]{:S(2)}) copy-start(bf16[128,1024]{1,0:T(8,128)(2,1)} %param.16) | copy-start | bytes 786436
  6.5 143.5 %copy-start.3 = (f32[8,128]{1,0:T(8,128)S(1)}, f32[8,128]{1,0:T(8,128)}, u32[]{:S(2)}) copy-start(f32[8,128]{1,0:T(8,128)} %param.20) | copy-start | bytes 12292
  6.5 144.4 %copy-start.5 = (bf16[128,1024]{1,0:T(8,128)(2,1)S(1)}, bf16[128,1024]{1,0:T(8,128)(2,1)}, u32[]{:S(2)}) copy-start(bf16[128,1024]{1,0:T(8,128)(2,1)} %param.19) | copy-start | bytes 786436
  6.5 144.4 %copy-start.6 = (f32[1024]{0:T(1024)S(1)}, f32[1024]{0:T(1024)}, u32[]{:S(2)}) copy-start(f32[1024]{0:T(1024)} %param.22) | copy-start | bytes 12292
  6.5 122.3 %all-gather.13.cloned.1.call-start = ((), (), s32[]{:S(2)}) async-start(), calls=%async_computation.6 | async-start | bytes 8912896 | tf_op jit(solution)/shard_map/all_gather | solution.py:13
  13.2 147.8 %reduce-scatter.3.cloned.1.call-start = ((), (), s32[]{:S(2)}) async-start(), calls=%async_computation.2 | async-start | bytes 786432 | tf_op jit(solution)/shard_map/reduce_scatter | solution.py:138
  149.2 7.5 %copy-start.4 = (bf16[3,1024]{1,0:T(4,128)(2,1)S(1)}, bf16[3,1024]{1,0:T(4,128)(2,1)}, u32[]{:S(2)}) copy-start(bf16[3,1024]{1,0:T(4,128)(2,1)} %param.24) | copy-start | bytes 18436
  149.2 15.3 %copy-start.2 = (bf16[128,1024]{1,0:T(8,128)(2,1)S(1)}, bf16[128,1024]{1,0:T(8,128)(2,1)}, u32[]{:S(2)}) copy-start(bf16[128,1024]{1,0:T(8,128)(2,1)} %param.15) | copy-start | bytes 786436
  154.7 151.6 %all-gather.15.cloned.1.call-start = ((), (), s32[]{:S(2)}) async-start(), calls=%async_computation.7 | async-start | bytes 12255232 | tf_op jit(solution)/shard_map/all_gather | solution.py:163
  155.5 293.1 %all-gather.9.cloned.1.call-start = ((), (), s32[]{:S(2)}) async-start(), calls=%async_computation.3 | async-start | bytes 12255232 | tf_op jit(solution)/shard_map/all_gather | solution.py:152
  156.1 434.7 %all-gather.11.cloned.1.call-start = ((), (), s32[]{:S(2)}) async-start(), calls=%async_computation.4 | async-start | bytes 12255232 | tf_op jit(solution)/shard_map/all_gather | solution.py:157
  156.6 453.7 %reduce-scatter.5.cloned.1.call-start = ((), (), s32[]{:S(2)}) async-start(), calls=%async_computation.5 | async-start | bytes 786432 | tf_op jit(solution)/shard_map/reduce_scatter | solution.py:166
  590.8 24.9 %copy-start.1 = (bf16[128,1024]{1,0:T(8,128)(2,1)S(1)}, bf16[128,1024]{1,0:T(8,128)(2,1)}, u32[]{:S(2)}) copy-start(bf16[128,1024]{1,0:T(8,128)(2,1)} %param.16) | copy-start | bytes 786436
Sparse Core Ops, SparseCore 0:
  13.4 115.4 all-gather.12
  154.9 6.0 reduce-scatter.2
  163.8 142.4 all-gather.14
  308.9 139.5 all-gather.8
  451.1 139.5 all-gather.10
  604.2 6.0 reduce-scatter.4
